TPU v7x, 32 devices: a whole 2x2x4 slice. The times are simulated.
32 devices in a mesh: sp: 8 (over z, y), tp: 4 (over x, core).
Axes of the slice: x: 2, y: 2, z: 4, core: 2. Of those that a mesh axis runs over, the one named last changes fastest.
Arguments:
- out_grad: bfloat16 [1024, 2048], P('sp', 'tp'), may hold values from -6 to 6
- route_ids: int32 [1024, 2], P('sp'), may hold values from 0 to 7, as said below
- route_weight: float32 [1024, 2], P('sp'), may hold values from 0.1 to 0.9
- expert_inputs: bfloat16 [8, 512, 2048], P('sp'), may hold values from -6 to 6
- gate_weight: bfloat16 [8, 2048, 3072], P('sp', None, 'tp'), may hold values from -0.125 to 0.125
- up_weight: bfloat16 [8, 2048, 3072], P('sp', None, 'tp'), may hold values from -0.125 to 0.125
- down_weight: bfloat16 [8, 3072, 2048], P('sp', 'tp'), may hold values from -0.109375 to 0.109375
- out_gate: bfloat16 [1024, 2048], P('sp', 'tp'), may hold values from -6 to 6
- in_gate: bfloat16 [1024, 2048], P('sp', 'tp'), may hold values from -6 to 6
- values: bfloat16 [1024, 2048], P('sp', 'tp'), may hold values from -6 to 6
- conv_out: bfloat16 [1024, 2048], P('sp', 'tp'), may hold values from -6 to 6
- conv_taps: bfloat16 [3, 2048], P(None, 'tp'), may hold values from -3.5 to 3.5
- proj_weight: bfloat16 [2048, 2048], P(None, 'tp'), may hold values from -0.125 to 0.125
Outputs:
- resid_grad: bfloat16 [1024, 2048], P('sp', 'tp')
- out_gate_grad: bfloat16 [1024, 2048], P('sp', 'tp')
- in_gate_grad: bfloat16 [1024, 2048], P('sp', 'tp')
- values_grad: bfloat16 [1024, 2048], P('sp', 'tp')
- proj_grad: float32 [2048, 2048], P('sp', 'tp')
- gate_grad: bfloat16 [8, 2048, 3072], P('sp', None, 'tp')
- up_grad: bfloat16 [8, 2048, 3072], P('sp', None, 'tp')
- down_grad: bfloat16 [8, 3072, 2048], P('sp', 'tp')
Inputs may be any that keep to these rules, and one draw needn't show every extreme that they name: `route_ids`: each row names two different experts. Among the rows of one device (aligned blocks of 128 rows) no expert is named more than 64 times, and in every draw one expert is named exactly 64 times in every block.
All inputs are finite; a program needn't handle non-finite values.
Results may differ from a plain program's by a relative error of at most 0.017.
Values may be sent and summed in bfloat16 or wider, within the bound.
A program may use at most 128 MiB of HBM per device.

v0:
```python
import functools
import math

import jax
import jax.numpy as jnp
from jax import lax
from jax.experimental import pallas as pl
from jax.experimental.pallas import tpu as pltpu
from jax.sharding import PartitionSpec as P

BF = jnp.bfloat16
F32 = jnp.float32
MESH = pl.DeviceIdType.MESH
VMEM = pl.BlockSpec(memory_space=pltpu.VMEM)
ANY = pl.BlockSpec(memory_space=pl.ANY)


def dot(left, right, dims):
    return lax.dot_general(left, right, ((dims[0], dims[1]), ((), ())), preferred_element_type=F32)


def remote(src, dst, send, recv, device):
    return pltpu.make_async_remote_copy(
        src_ref=src, dst_ref=dst, send_sem=send, recv_sem=recv, device_id=device, device_id_type=MESH
    )


def hail(n_sp, me, partners):
    barrier = pltpu.get_barrier_semaphore()
    for d in range(1, n_sp):
        pl.semaphore_signal(
            barrier, inc=1, device_id={"sp": lax.rem(me + d, n_sp)}, device_id_type=MESH
        )
    for tp in partners:
        pl.semaphore_signal(barrier, inc=1, device_id={"tp": tp}, device_id_type=MESH)


def met(n_sp, partners):
    pl.semaphore_wait(pltpu.get_barrier_semaphore(), n_sp - 1 + len(partners))


class Exchange:
    def __init__(self, n_sp, me, tp, sib, far, src_at, dst_at, sems):
        self.n_sp, self.me, self.tp, self.sib, self.far = n_sp, me, tp, sib, far
        self.src_at, self.dst_at, self.sems = src_at, dst_at, sems

    def source(self, d):
        return lax.rem(self.me - d + self.n_sp, self.n_sp)

    def sp_copy(self, d):
        to = lax.rem(self.me + d, self.n_sp)
        return remote(
            self.src_at(to), self.dst_at(self.tp, self.me),
            self.sems.at[0, d], self.sems.at[1, d], {"sp": to},
        )

    def far_copy(self, d):
        place = self.dst_at(self.tp, self.source(d))
        return remote(place, place, self.sems.at[2, d], self.sems.at[3, d], {"tp": self.far})

    def sib_copy(self, d):
        place = self.dst_at(self.tp, self.source(d))
        return remote(place, place, self.sems.at[4, d], self.sems.at[5, d], {"tp": self.sib})

    def hand_copy(self, d):
        place = self.dst_at(self.far, self.source(d))
        return remote(place, place, self.sems.at[6, d], self.sems.at[7, d], {"tp": self.sib})

    def start(self):
        for d in range(1, self.n_sp):
            self.sp_copy(d).start()
        own = pltpu.make_async_copy(
            self.src_at(self.me), self.dst_at(self.tp, self.me), self.sems.at[0, 0]
        )
        own.start()
        own.wait()
        self.far_copy(0).start()
        self.sib_copy(0).start()

    def spread(self, d):
        self.sp_copy(d).wait_recv()
        self.far_copy(d).start()
        self.sib_copy(d).start()

    def hand(self, d):
        self.far_copy(d).wait_recv()
        self.hand_copy(d).start()

    def finish(self):
        n = self.n_sp

        @pl.loop(0, n)
        def _(d):
            self.far_copy(d).wait_send()
            self.sib_copy(d).wait_send()
            self.sib_copy(d).wait_recv()
            self.hand_copy(d).wait_send()
            self.hand_copy(d).wait_recv()

        @pl.loop(1, n)
        def _(d):
            self.sp_copy(d).wait_send()


def expert_kernel(
    n_sp, n_tp, experts,
    og_ref, ids_ref, rw_ref, x_hbm, gw_hbm, uw_hbm, dw_hbm,
    routed, hidden, dall, resid, rfull, quarter,
    x, w, dw, pre, outgoing, parts, from_sib, far_out, far_in, total, final, back, disp,
    load_sems, ex_sems, sib_sems, far_sems, ret_sems, gat_sems,
):
    me, tp = lax.axis_index("sp"), lax.axis_index("tp")
    sib = tp + 1 - 2 * lax.rem(tp, 2)
    far = lax.rem(tp + n_tp // 2, n_tp)
    tokens, chan = og_ref.shape
    slots, width = x.shape
    hid = dw.shape[0]
    cap = slots // n_sp
    local = experts // n_sp

    loads = [
        pltpu.make_async_copy(x_hbm.at[0], x, load_sems.at[0]),
        pltpu.make_async_copy(gw_hbm.at[0], w.at[:, pl.ds(0, hid)], load_sems.at[1]),
        pltpu.make_async_copy(uw_hbm.at[0], w.at[:, pl.ds(hid, hid)], load_sems.at[2]),
        pltpu.make_async_copy(dw_hbm.at[0], dw, load_sems.at[3]),
    ]
    for load in loads:
        load.start()

    hail(n_sp, me, (sib, far))
    ids = ids_ref[...]
    id0, id1 = ids[:, 0:1], ids[:, 1:2]
    rw = rw_ref[...]
    lanes = lax.broadcasted_iota(jnp.int32, (tokens, 128), 1)
    hit0 = jnp.where(id0 == lanes, 1.0, 0.0).astype(F32)
    hit1 = jnp.where(id1 == lanes, 1.0, 0.0).astype(F32)
    rows = lax.broadcasted_iota(jnp.int32, (tokens, tokens), 0)
    cols = lax.broadcasted_iota(jnp.int32, (tokens, tokens), 1)
    earlier = jnp.where(rows > cols, 1.0, 0.0).astype(BF)
    counts = dot(earlier, (hit0 + hit1).astype(BF), ((1,), (0,)))
    rank0 = jnp.sum(counts * hit0, axis=1, keepdims=True)
    rank1 = jnp.sum(counts * hit1, axis=1, keepdims=True)
    slot0 = id0.astype(F32) * float(cap) + rank0
    slot1 = id1.astype(F32) * float(cap) + rank1
    places = lax.broadcasted_iota(jnp.int32, (tokens, experts * cap), 1).astype(F32)
    d0 = jnp.where(slot0 == places, 1.0, 0.0).astype(BF)
    d1 = jnp.where(slot1 == places, 1.0, 0.0).astype(BF)
    disp[...] = d0 + d1
    og = og_ref[...].astype(F32)
    sent = dot(d0, (rw[:, 0:1] * og).astype(BF), ((0,), (0,)))
    sent = sent + dot(d1, (rw[:, 1:2] * og).astype(BF), ((0,), (0,)))
    outgoing[...] = sent.astype(BF)

    met(n_sp, (sib, far))
    ex = Exchange(
        n_sp, me, tp, sib, far,
        lambda k: outgoing.at[pl.ds(pl.multiple_of(k * cap, cap), cap), :],
        lambda j, s: routed.at[
            pl.ds(pl.multiple_of(s * cap, cap), cap), pl.ds(pl.multiple_of(j * chan, chan), chan)
        ],
        ex_sems,
    )
    ex.start()
    for load in loads:
        load.wait()
    tile = 256
    pre_tiles = 2 * hid // tile
    both = min(pre_tiles, n_sp - 1)

    def pre_dot(t):
        at = pl.ds(pl.multiple_of(t * tile, tile), tile)
        pre[:, at] = dot(x[...], w[:, at], ((1,), (0,)))

    @pl.loop(0, both)
    def _(t):
        ex.spread(t + 1)
        pre_dot(t)
        ex.hand(t)

    if both < pre_tiles:
        pl.loop(both, pre_tiles)(pre_dot)
    if both < n_sp - 1:
        pl.loop(both + 1, n_sp)(ex.spread)
    pl.loop(both, n_sp)(ex.hand)
    ex.finish()

    @pl.loop(0, hid // tile)
    def _(t):
        at = pl.ds(pl.multiple_of(t * tile, tile), tile)
        up_at = pl.ds(pl.multiple_of(hid + t * tile, tile), tile)
        d_hidden = dot(routed[...], dw[at, :], ((1,), (1,)))
        gate, up = pre[:, at], pre[:, up_at]
        sig = jax.nn.sigmoid(gate)
        act = gate * sig
        hidden[:, at] = (act * up).astype(BF)
        dall[:, at] = (d_hidden * up * sig * (1.0 + gate * (1.0 - sig))).astype(BF)
        dall[:, up_at] = (d_hidden * act).astype(BF)

    def back_part(block, place):
        @pl.loop(0, chan // tile)
        def _(t):
            at = pl.ds(pl.multiple_of(block * chan + t * tile, tile), tile)
            value = dot(dall[...], w[at, :], ((1,), (1,)))
            parts[place, :, pl.ds(pl.multiple_of(t * tile, tile), tile)] = value.astype(BF)

    far_sib = lax.rem(sib + n_tp // 2, n_tp)
    sib_copies = [
        remote(parts.at[2 * i], from_sib.at[i], sib_sems.at[0, i], sib_sems.at[1, i], {"tp": sib})
        for i in range(2)
    ]

    def at_rows(d):
        s = lax.rem(me + d, n_sp)
        return pl.ds(pl.multiple_of(s * cap, cap), cap)

    def far_copy(d):
        return remote(
            far_out.at[at_rows(d), :], far_in.at[at_rows(d), :],
            far_sems.at[0, lax.rem(d, n_sp)], far_sems.at[1, lax.rem(d, n_sp)], {"tp": far},
        )

    def ret_copy(d):
        mine = pl.ds(pl.multiple_of(me * cap, cap), cap)
        return remote(
            final.at[at_rows(d), :], back.at[mine, :],
            ret_sems.at[0, d], ret_sems.at[1, d], {"sp": lax.rem(me + d, n_sp)},
        )

    back_part(far_sib, 0)
    sib_copies[0].start()
    back_part(far, 1)
    sib_copies[0].wait_recv()

    @pl.loop(1, n_sp + 1)
    def _(d):
        at = at_rows(d)
        far_out[at, :] = (parts[1, at, :].astype(F32) + from_sib[0, at, :].astype(F32)).astype(BF)
        far_copy(d).start()

    back_part(sib, 2)
    sib_copies[1].start()
    back_part(tp, 3)
    sib_copies[1].wait_recv()
    total[...] = parts[3].astype(F32) + from_sib[1].astype(F32)

    @pl.loop(1, n_sp)
    def _(d):
        at = at_rows(d)
        far_copy(d).wait_recv()
        final[at, :] = (total[at, :] + far_in[at, :].astype(F32)).astype(BF)
        ret_copy(d).start()

    far_copy(n_sp).wait_recv()
    at = at_rows(0)
    back[at, :] = (total[at, :] + far_in[at, :].astype(F32)).astype(BF)

    @pl.loop(1, n_sp)
    def _(d):
        ret_copy(d).wait_recv()

    value = (og_ref[...].astype(F32) + dot(disp[...], back[...], ((1,), (0,)))).astype(BF)
    resid[...] = value
    rfull[tp] = value
    near = remote(rfull.at[tp], rfull.at[tp], gat_sems.at[0], gat_sems.at[1], {"tp": sib})
    away = remote(rfull.at[tp], rfull.at[tp], gat_sems.at[2], gat_sems.at[3], {"tp": far})
    away.start()
    near.start()
    away.wait_recv()
    hand = remote(rfull.at[far], rfull.at[far], gat_sems.at[4], gat_sems.at[5], {"tp": sib})
    hand.start()
    near.wait_recv()
    hand.wait_recv()
    share = tokens // n_tp
    piece = width // n_sp
    for k in range(n_sp):
        block, first = divmod(k * piece, chan)
        quarter[k] = rfull[
            block, pl.ds(pl.multiple_of(tp * share, share), share), first:first + piece
        ]
    near.wait_send()
    away.wait_send()
    hand.wait_send()
    for copy in sib_copies:
        copy.wait_send()

    @pl.loop(1, n_sp)
    def _(d):
        far_copy(d).wait_send()
        ret_copy(d).wait_send()

    far_copy(n_sp).wait_send()


def mixer_kernel(
    n_sp, n_tp,
    quarter, rfull, pw_hbm, og_ref, ig_ref, val_ref, conv_ref, taps_ref,
    columns, og_out, ig_out, val_out,
    pw, edge_out, edge_in, ex_sems, halo_sems, load_sem,
):
    me, tp = lax.axis_index("sp"), lax.axis_index("tp")
    sib = tp + 1 - 2 * lax.rem(tp, 2)
    far = lax.rem(tp + n_tp // 2, n_tp)
    tokens, chan = og_ref.shape
    load = pltpu.make_async_copy(pw_hbm, pw, load_sem)
    load.start()
    hail(n_sp, me, (sib, far))
    met(n_sp, (sib, far))
    ex = Exchange(
        n_sp, me, tp, sib, far, lambda k: quarter.at[k], lambda j, s: columns.at[s, j], ex_sems
    )
    ex.start()
    load.wait()
    mix = dot(rfull[0], pw[0:chan, :], ((1,), (0,)))
    for j in range(1, n_tp):
        mix = mix + dot(rfull[j], pw[j * chan:(j + 1) * chan, :], ((1,), (0,)))
    og_out[...] = (mix * conv_ref[...].astype(F32)).astype(BF)
    grad = (mix * og_ref[...].astype(F32)).astype(BF).astype(F32)
    edge_out[0] = jnp.broadcast_to(grad[tokens - 1:tokens, :], edge_out.shape[1:])
    edge_out[1] = jnp.broadcast_to(grad[0:1, :], edge_out.shape[1:])
    sides = [lax.rem(me + 1, n_sp), lax.rem(me + n_sp - 1, n_sp)]
    halos = [
        remote(edge_out.at[i], edge_in.at[i], halo_sems.at[0, i], halo_sems.at[1, i], {"sp": sides[i]})
        for i in range(2)
    ]
    for halo in halos:
        halo.start()
    pl.loop(1, n_sp)(ex.spread)
    pl.loop(0, n_sp)(ex.hand)
    for halo in halos:
        halo.wait()
    before = jnp.where(me == 0, 0.0, edge_in[0, 0:1, :])
    after = jnp.where(me == n_sp - 1, 0.0, edge_in[1, 0:1, :])
    row = lax.broadcasted_iota(jnp.int32, (tokens, chan), 0)
    prev = jnp.where(row == 0, before, pltpu.roll(grad, 1, 0))
    following = jnp.where(row == tokens - 1, after, pltpu.roll(grad, tokens - 1, 0))
    taps = taps_ref[...].astype(F32)
    value_grad = following * taps[0:1, :] + grad * taps[1:2, :] + prev * taps[2:3, :]
    ig_out[...] = (value_grad * val_ref[...].astype(F32)).astype(BF)
    val_out[...] = (value_grad * ig_ref[...].astype(F32)).astype(BF)
    ex.finish()


def in_grads(scale, x, d, gate, up):
    hid = gate.shape[-1]
    left = x[0].T
    gate[0] = (dot(left, d[:, :hid], ((1,), (0,))) * scale).astype(BF)
    up[0] = (dot(left, d[:, hid:], ((1,), (0,))) * scale).astype(BF)


def out_grads(scale, h, r, down):
    down[0] = (dot(h[...].T, r[...], ((1,), (0,))) * scale).astype(BF)


def per_device(
    out_grad, route_ids, route_weight, expert_inputs, gate_weight, up_weight, down_weight,
    out_gate, in_gate, values, conv_out, conv_taps, proj_weight,
):
    n_sp, n_tp = lax.axis_size("sp"), lax.axis_size("tp")
    tokens, chan = out_grad.shape
    local, slots, width = expert_inputs.shape
    hid = gate_weight.shape[2]
    assert local == 1 and n_tp == 4
    share, piece = tokens // n_tp, width // n_sp
    dma = pltpu.SemaphoreType.DMA
    mixed_in = (out_gate.astype(F32) * conv_out.astype(F32)).astype(BF)
    mixed_all = lax.all_gather(mixed_in, "sp", axis=0, tiled=True)

    routed, hidden, dall, resid, rfull, quarter = pl.pallas_call(
        functools.partial(expert_kernel, n_sp, n_tp, n_sp * local),
        out_shape=[
            jax.ShapeDtypeStruct((slots, width), BF),
            jax.ShapeDtypeStruct((slots, hid), BF),
            jax.ShapeDtypeStruct((slots, 2 * hid), BF),
            jax.ShapeDtypeStruct((tokens, chan), BF),
            jax.ShapeDtypeStruct((n_tp, tokens, chan), BF),
            jax.ShapeDtypeStruct((n_sp, share, piece), BF),
        ],
        in_specs=[VMEM] * 3 + [ANY] * 4,
        out_specs=[VMEM] * 6,
        scratch_shapes=[
            pltpu.VMEM((slots, width), BF),
            pltpu.VMEM((width, 2 * hid), BF),
            pltpu.VMEM((hid, width), BF),
            pltpu.VMEM((slots, 2 * hid), F32),
            pltpu.VMEM((slots, chan), BF),
            pltpu.VMEM((4, slots, chan), BF),
            pltpu.VMEM((2, slots, chan), BF),
            pltpu.VMEM((slots, chan), BF),
            pltpu.VMEM((slots, chan), BF),
            pltpu.VMEM((slots, chan), F32),
            pltpu.VMEM((slots, chan), BF),
            pltpu.VMEM((slots, chan), BF),
            pltpu.VMEM((tokens, slots), BF),
            dma((4,)), dma((8, n_sp)), dma((2, 2)), dma((2, n_sp)), dma((2, n_sp)), dma((6,)),
        ],
        compiler_params=pltpu.CompilerParams(
            collective_id=0, has_side_effects=True, vmem_limit_bytes=48 * 2**20
        ),
        name="experts",
    )(out_grad, route_ids, route_weight, expert_inputs, gate_weight, up_weight, down_weight)

    columns, out_gate_grad, in_gate_grad, values_grad = pl.pallas_call(
        functools.partial(mixer_kernel, n_sp, n_tp),
        out_shape=[
            jax.ShapeDtypeStruct((n_sp, n_tp, share, piece), BF),
            jax.ShapeDtypeStruct((tokens, chan), BF),
            jax.ShapeDtypeStruct((tokens, chan), BF),
            jax.ShapeDtypeStruct((tokens, chan), BF),
        ],
        in_specs=[VMEM, VMEM, ANY] + [VMEM] * 5,
        out_specs=[VMEM] * 4,
        scratch_shapes=[
            pltpu.VMEM(proj_weight.shape, BF),
            pltpu.VMEM((2, 8, chan), F32),
            pltpu.VMEM((2, 8, chan), F32),
            dma((8, n_sp)), dma((2, 2)), dma,
        ],
        compiler_params=pltpu.CompilerParams(
            collective_id=1, has_side_effects=True, vmem_limit_bytes=32 * 2**20
        ),
        name="mixer",
    )(quarter, rfull, proj_weight, out_gate, in_gate, values, conv_out, conv_taps)

    slot_scale = 1.0 / math.sqrt(slots)
    wide = 512
    gate_grad, up_grad = pl.pallas_call(
        functools.partial(in_grads, slot_scale),
        grid=(width // wide,),
        in_specs=[
            pl.BlockSpec((1, slots, wide), lambda i: (0, 0, i)),
            pl.BlockSpec((slots, 2 * hid), lambda i: (0, 0)),
        ],
        out_specs=[pl.BlockSpec((1, wide, hid), lambda i: (0, i, 0))] * 2,
        out_shape=[jax.ShapeDtypeStruct((1, width, hid), BF)] * 2,
        name="in_grads",
    )(expert_inputs, dall)
    down_grad = pl.pallas_call(
        functools.partial(out_grads, slot_scale),
        grid=(hid // 256,),
        in_specs=[
            pl.BlockSpec((slots, 256), lambda i: (0, i)),
            pl.BlockSpec((slots, width), lambda i: (0, 0)),
        ],
        out_specs=pl.BlockSpec((1, 256, width), lambda i: (0, i, 0)),
        out_shape=jax.ShapeDtypeStruct((1, hid, width), BF),
        name="out_grads",
    )(hidden, routed)
    proj_sum = lax.dot_general(
        columns.reshape(n_sp * tokens, piece), mixed_all,
        (((0,), (0,)), ((), ())), preferred_element_type=F32,
    )
    proj_grad = proj_sum * (1.0 / math.sqrt(tokens * n_sp))
    return (
        resid, out_gate_grad, in_gate_grad, values_grad, proj_grad, gate_grad, up_grad, down_grad,
    )


def solution(mesh):
    rows = P("sp", "tp")
    in_specs = (
        rows, P("sp", None), P("sp", None), P("sp", None, None), P("sp", None, "tp"),
        P("sp", None, "tp"), P("sp", "tp", None), rows, rows, rows, rows, P(None, "tp"), P(None, "tp"),
    )
    out_specs = (
        rows, rows, rows, rows, rows, P("sp", None, "tp"), P("sp", None, "tp"), P("sp", "tp", None),
    )
    return jax.shard_map(
        per_device, mesh=mesh, in_specs=in_specs, out_specs=out_specs, check_vma=False
    )
```

profile of v0, /device:TPU:7, one launch (start us, length us, event | category | flops | bytes accessed | tf_op | source)
XLA Modules:
  0.0 108.3 jit_solution(9440159171710733266)
XLA Ops:
  7.2 0.0 all-gather.2.cloned.1.call-start
  7.2 1.7 %multiply_convert_fusion = bf16[128,512]{1,0:T(8,128)(2,1)} fusion(bf16[128,512]{1,0:T(8,128)(2,1)} %conv_ref.1, bf16[128,512]{1,0:T(8,128)(2,1)} %og_ref.3), kind=kLoop, calls=%fused_computation.1 | loop fusion | flops 262144 | bytes 393216 | tf_op jit(solution)/shard_map/convert_element_type | solution.py:365
  8.9 0.0 all-gather.2.cloned.1.call-update
  8.9 0.8 copy.21.ids_ref
  9.7 0.8 copy.22.rw_ref
  10.5 0.0 copy-start.6
  10.5 0.9 copy-done.6
  11.4 0.0 copy-start.1
  11.4 0.0 copy-start.4
  11.4 0.0 copy-start.5
  11.4 0.0 copy-start.7
  11.4 0.0 copy-start.8
  11.4 0.0 copy-start.9
  11.4 57.7 %experts.1 = (bf16[512,2048]{1,0:T(8,128)(2,1)S(1)}, bf16[512,768]{1,0:T(8,128)(2,1)S(1)}, bf16[512,1536]{1,0:T(8,128)(2,1)S(1)}, bf16[128,512]{1,0:T(8,128)(2,1...) custom-call(bf16[128,512]{1,0:T(8,128)(2,1)S(1)} %copy-done.6, s32[128,2]{1,0:T(8,128)S(1)} %copy.21.ids_ref, ...), custom_call_target="tpu_custom_call" | custom-call | tf_op jit(solution)/shard_map/experts/pallas_call | solution.py:368
  69.2 0.0 copy-start
  69.2 1.3 %copy-done = bf16[512,2048]{1,0:T(8,128)(2,1)} copy-done((bf16[512,2048]{1,0:T(8,128)(2,1)}, bf16[512,2048]{1,0:T(8,128)(2,1)S(1)}, u32[]{:S(2)}) %copy-start) | copy-done | bytes 2097176
  70.5 0.0 copy-done.1
  70.5 0.0 copy-done.4
  70.5 0.0 copy-done.5
  70.5 0.0 copy-done.7
  70.5 0.0 copy-done.8
  70.5 0.0 copy-done.9
  70.5 13.6 %mixer.1 = (bf16[8,4,32,256]{3,2,1,0:T(8,128)(2,1)S(1)}, bf16[128,512]{1,0:T(8,128)(2,1)S(1)}, bf16[128,512]{1,0:T(8,128)(2,1)S(1)}, bf16[128,512]{1,0:T(8,128)(2,1)S(1)}) custom-call(bf16[8,32,256]{2,1,0:T(8,128)(2,1)S(1)} %get-tuple-element.21.quarter, bf16[4,128,512]{2,1,0:T(8,128)(2,1)S(1)} %get-tuple-element.22.rfull, bf16[2048,512]{1,0:T(8,128)(2,1)S(1)} %copy-done.1, ...), custom_call_target="tpu_custom_call" | custom-call | tf_op jit(solution)/shard_map/mixer/pallas_call | solution.py:402
  84.2 0.0 copy-done.2
  84.2 0.0 copy-done.3
  84.2 6.9 %in_grads.1 = (bf16[1,2048,768]{2,1,0:T(8,128)(2,1)}, bf16[1,2048,768]{2,1,0:T(8,128)(2,1)}) custom-call(bf16[1,512,2048]{2,1,0:T(8,128)(2,1)} %x.1, bf16[512,1536]{1,0:T(8,128)(2,1)} %copy-done.2), custom_call_target="tpu_custom_call" | custom-call | tf_op jit(solution)/shard_map/in_grads/pallas_call | solution.py:426
  91.1 5.3 %out_grads.1 = bf16[1,768,2048]{2,1,0:T(8,128)(2,1)} custom-call(bf16[512,768]{1,0:T(8,128)(2,1)} %copy-done.3, bf16[512,2048]{1,0:T(8,128)(2,1)} %copy-done), custom_call_target="tpu_custom_call" | custom-call | tf_op jit(solution)/shard_map/out_grads/pallas_call | solution.py:437
  96.4 2.5 %convolution_multiply_fusion = f32[256,512]{1,0:T(8,128)} fusion(bf16[1024,256]{1,0:T(8,128)(2,1)S(1)} %bitcast.3, bf16[1024,512]{1,0:T(8,128)(2,1)} %all-gather.2.cloned.1.call-done), kind=kOutput, calls=%fused_computation | convolution fusion | flops 268566528 | bytes 2097152 | tf_op jit(solution)/shard_map/dot_general | solution.py:448
  98.9 0.7 copy.27
  99.5 0.7 copy.28
  100.2 0.7 copy.29
  100.8 0.7 copy.30
  (3 shorter events, 0.0 us)
Async XLA Ops:
  7.2 89.2 %all-gather.2.cloned.1.call-start = ((), (), s32[]{:S(2)}) async-start(), calls=%async_computation | async-start | bytes 1179648 | tf_op jit(solution)/shard_map/all_gather | solution.py:366
  10.5 0.9 copy-start.6
  11.4 59.1 %copy-start.1 = (bf16[2048,512]{1,0:T(8,128)(2,1)S(1)}, bf16[2048,512]{1,0:T(8,128)(2,1)}, u32[]{:S(2)}) copy-start(bf16[2048,512]{1,0:T(8,128)(2,1)} %pw_hbm.1) | copy-start | bytes 6291460
  11.4 59.1 %copy-start.4 = (bf16[128,512]{1,0:T(8,128)(2,1)S(1)}, bf16[128,512]{1,0:T(8,128)(2,1)}, u32[]{:S(2)}) copy-start(bf16[128,512]{1,0:T(8,128)(2,1)} %og_ref.3) | copy-start | bytes 393220
  11.4 59.1 %copy-start.5 = (bf16[128,512]{1,0:T(8,128)(2,1)S(1)}, bf16[128,512]{1,0:T(8,128)(2,1)}, u32[]{:S(2)}) copy-start(bf16[128,512]{1,0:T(8,128)(2,1)} %conv_ref.1) | copy-start | bytes 393220
  11.4 59.1 %copy-start.7 = (bf16[128,512]{1,0:T(8,128)(2,1)S(1)}, bf16[128,512]{1,0:T(8,128)(2,1)}, u32[]{:S(2)}) copy-start(bf16[128,512]{1,0:T(8,128)(2,1)} %ig_ref.1) | copy-start | bytes 393220
  11.4 59.1 %copy-start.8 = (bf16[128,512]{1,0:T(8,128)(2,1)S(1)}, bf16[128,512]{1,0:T(8,128)(2,1)}, u32[]{:S(2)}) copy-start(bf16[128,512]{1,0:T(8,128)(2,1)} %val_ref.1) | copy-start | bytes 393220
  11.4 59.1 %copy-start.9 = (bf16[3,512]{1,0:T(4,128)(2,1)S(1)}, bf16[3,512]{1,0:T(4,128)(2,1)}, u32[]{:S(2)}) copy-start(bf16[3,512]{1,0:T(4,128)(2,1)} %taps_ref.1) | copy-start | bytes 9220
  69.2 1.3 %copy-start = (bf16[512,2048]{1,0:T(8,128)(2,1)}, bf16[512,2048]{1,0:T(8,128)(2,1)S(1)}, u32[]{:S(2)}) copy-start(bf16[512,2048]{1,0:T(8,128)(2,1)S(1)} %get-tuple-element.31.r) | copy-start | bytes 6291460
  70.5 13.7 %copy-start.2 = (bf16[512,1536]{1,0:T(8,128)(2,1)}, bf16[512,1536]{1,0:T(8,128)(2,1)S(1)}, u32[]{:S(2)}) copy-start(bf16[512,1536]{1,0:T(8,128)(2,1)S(1)} %get-tuple-element.27.d) | copy-start | bytes 4718596
  70.5 13.7 %copy-start.3 = (bf16[512,768]{1,0:T(8,128)(2,1)}, bf16[512,768]{1,0:T(8,128)(2,1)S(1)}, u32[]{:S(2)}) copy-start(bf16[512,768]{1,0:T(8,128)(2,1)S(1)} %get-tuple-element.30.h) | copy-start | bytes 2359300
Sparse Core Ops, SparseCore 0:
  10.7 50.9 all-gather.1
where the time goes:
time: 110 us; the launch traced here: 108 us
  Pallas kernels  83.5 us (76%)
  between operations  14.1 us (13%)
  local copies, waits for them, and re-layouts  6.45 us (6%)
  matrix products  2.47 us (2%)
  other arithmetic  1.66 us (2%)
    pallas_call x1, Pallas kernels, per_device(): pl.pallas_call(functools.partial(expert_kernel, n_sp, n_tp, n_sp * local)...  57.7 us
    pallas_call x1, Pallas kernels, per_device(): pl.pallas_call(functools.partial(mixer_kernel, n_sp, n_tp), out_shape=[ja...  13.6 us
    pallas_call x1, Pallas kernels, per_device(): pl.pallas_call(functools.partial(in_grads, slot_scale), grid=(width // wi...  6.92 us
    unnamed x26, local copies, waits for them, and re-layouts  6.45 us
    pallas_call x1, Pallas kernels, per_device(): pl.pallas_call(functools.partial(out_grads, slot_scale), grid=(hid // 256...  5.28 us
    dot_general x1, matrix products, per_device(): lax.dot_general(columns.reshape(n_sp * tokens, piece), mixed_all, (((0,),...  2.47 us
  transfers between devices with their start and end apart: 1, of which 0 were waited for; matrix products, arithmetic and copies ran while one was open for 1% of the time, Pallas kernels for 77%

commit v1 on v0

v1 whole, which is shorter than its diff:
```python
import functools
import math

import jax
import jax.numpy as jnp
from jax import lax
from jax.experimental import pallas as pl
from jax.experimental.pallas import tpu as pltpu
from jax.sharding import PartitionSpec as P

BF = jnp.bfloat16
F32 = jnp.float32
MESH = pl.DeviceIdType.MESH
VMEM = pl.BlockSpec(memory_space=pltpu.VMEM)
HBM = pl.BlockSpec(memory_space=pltpu.HBM)
NT = ((1,), (1,))
NN = ((1,), (0,))


def dot(left, right, dims):
    return lax.dot_general(left, right, (dims, ((), ())), preferred_element_type=F32)


def remote(src, dst, send, recv, device):
    return pltpu.make_async_remote_copy(
        src_ref=src, dst_ref=dst, send_sem=send, recv_sem=recv, device_id=device, device_id_type=MESH
    )


def span(index, size):
    return pl.ds(pl.multiple_of(index * size, size), size)


def flip(s, m, n):
    out, bit = 0, 1
    while bit < n:
        out = out + bit * lax.rem(lax.div(s, bit) + (m // bit if isinstance(m, int) else lax.div(m, bit)), 2)
        bit *= 2
    return out


def low(m):
    return m & -m


def layer_kernel(
    n_sp, n_tp, experts, slot_scale,
    grad_hbm, ids_hbm, rw_hbm, x_hbm, gw_hbm, uw_hbm, dw_hbm,
    og_hbm, ig_hbm, val_hbm, conv_hbm, taps_hbm, pw_hbm,
    resid, og_out, ig_out, val_out, columns, zall, ggrad, ugrad, dgrad,
    grad, ids, rw, x, w, dw, og, ig, val, conv, taps, pw,
    xt, pre, routed, hidden, dall, outgoing, parts, from_sib, far_out, far_in, total, final, back, disp,
    rfull, pieces, edge_out, edge_in,
    load_sems, ex_sems, sib_sems, far_sems, ret_sems, gat_sems, z_sems, e_sems, halo_sems,
):
    me, tp = lax.axis_index("sp"), lax.axis_index("tp")
    core = lax.rem(tp, 2)
    sib = tp + 1 - 2 * core
    far = lax.rem(tp + n_tp // 2, n_tp)
    far_sib = lax.rem(sib + n_tp // 2, n_tp)
    tokens, chan = grad.shape
    slots, width = x.shape
    hid = dw.shape[0]
    cap = slots // n_sp
    half, quarter = n_sp // 2, n_sp // 4
    piece = width // n_sp
    per_block = chan // piece
    share = tokens // 2
    tile = 256

    pairs = [
        (grad_hbm, grad), (ids_hbm, ids), (rw_hbm, rw), (og_hbm, og), (conv_hbm, conv),
        (x_hbm.at[0], x), (gw_hbm.at[0], w.at[:, pl.ds(0, hid)]), (uw_hbm.at[0], w.at[:, pl.ds(hid, hid)]),
        (dw_hbm.at[0], dw), (ig_hbm, ig), (val_hbm, val), (taps_hbm, taps), (pw_hbm, pw),
    ]
    loads = [pltpu.make_async_copy(a, b, load_sems.at[i]) for i, (a, b) in enumerate(pairs)]
    for load in loads[:3]:
        load.start()
    barrier = pltpu.get_barrier_semaphore()
    for m in range(1, n_sp):
        pl.semaphore_signal(barrier, inc=1, device_id={"sp": flip(me, m, n_sp)}, device_id_type=MESH)
    for other in (sib, far):
        pl.semaphore_signal(barrier, inc=1, device_id={"tp": other}, device_id_type=MESH)
    for load in loads[3:]:
        load.start()
    for load in loads[:3]:
        load.wait()

    id0, id1 = ids[0:1, :], ids[1:2, :]
    names = lax.broadcasted_iota(jnp.int32, (experts, tokens), 0)
    hit0 = jnp.where(id0 == names, 1.0, 0.0).astype(F32)
    hit1 = jnp.where(id1 == names, 1.0, 0.0).astype(F32)
    rows = lax.broadcasted_iota(jnp.int32, (tokens, tokens), 0)
    cols = lax.broadcasted_iota(jnp.int32, (tokens, tokens), 1)
    earlier = jnp.where(rows < cols, 1.0, 0.0).astype(BF)
    counts = dot((hit0 + hit1).astype(BF), earlier, NN)
    slot0 = id0.astype(F32) * float(cap) + jnp.sum(counts * hit0, axis=0, keepdims=True)
    slot1 = id1.astype(F32) * float(cap) + jnp.sum(counts * hit1, axis=0, keepdims=True)
    places = lax.broadcasted_iota(jnp.int32, (experts * cap, tokens), 0).astype(F32)
    at0, at1 = slot0 == places, slot1 == places
    weight = jnp.sum(
        jnp.where(at0, rw[0:1, :], 0.0) + jnp.where(at1, rw[1:2, :], 0.0), axis=1, keepdims=True
    )
    chosen = (jnp.where(at0, 1.0, 0.0) + jnp.where(at1, 1.0, 0.0)).astype(BF)
    outgoing[...] = (dot(chosen, grad[...], NN) * weight).astype(BF)

    pl.semaphore_wait(barrier, n_sp + 1)

    def row_at(s):
        return span(s, cap)

    def place(j, s):
        return routed.at[row_at(s), span(j, chan)]

    def sp_copy(m):
        to = flip(me, m, n_sp)
        return remote(
            outgoing.at[row_at(to), :], place(tp, me), ex_sems.at[0, m], ex_sems.at[1, m], {"sp": to}
        )

    def far_share(m):
        at = place(tp, flip(me, m, n_sp))
        return remote(at, at, ex_sems.at[2, m], ex_sems.at[3, m], {"tp": far})

    def sib_share(m):
        at = place(tp, flip(me, m, n_sp))
        return remote(at, at, ex_sems.at[4, m], ex_sems.at[5, m], {"tp": sib})

    def hand_share(m):
        at = place(far, flip(me, m, n_sp))
        return remote(at, at, ex_sems.at[6, m], ex_sems.at[7, m], {"tp": sib})

    def spread(m):
        sp_copy(m).wait_recv()
        far_share(m).start()
        sib_share(m).start()

    def hand(m):
        far_share(m).wait_recv()
        hand_share(m).start()

    @pl.loop(1, n_sp)
    def _(m):
        sp_copy(m).start()

    own = pltpu.make_async_copy(outgoing.at[row_at(me), :], place(tp, me), ex_sems.at[0, 0])
    own.start()
    own.wait()
    far_share(0).start()
    sib_share(0).start()

    loads[3].wait()
    loads[4].wait()
    zall[me] = (og[...].astype(F32) * conv[...].astype(F32)).astype(BF)
    disp[...] = chosen.T

    def z_copy(result, bit):
        block = flip(me, result - bit, n_sp)
        return remote(
            zall.at[block], zall.at[block], z_sems.at[0, result], z_sems.at[1, result],
            {"sp": flip(me, bit, n_sp)},
        )

    def z_send(m):
        bit = low(m) // 2 if m else half // 2
        while bit:
            z_copy(m + bit, bit).start()
            bit //= 2

    def z_forward(m):
        if low(m) > 1:
            z_copy(m, low(m)).wait_recv()
            z_send(m)

    z_send(0)

    def pre_dot(t):
        at = span(t, tile)
        pre[:, at] = dot(x[...], w[:, at], NN)

    for load in loads[5:8]:
        load.wait()
    pre_tiles = 2 * hid // tile
    first = min(pre_tiles, half)
    spread(1)

    @pl.loop(0, first)
    def _(t):
        spread(t + 2)
        pre_dot(t)
        hand(t)

    if first < pre_tiles:
        pl.loop(first, pre_tiles)(pre_dot)

    if first < half:
        @pl.loop(first, half)
        def _(t):
            spread(t + 2)
            hand(t)

    @pl.loop(0, half)
    def _(m):
        sib_share(m).wait_recv()
        hand_share(m).wait_recv()

    loads[8].wait()

    def hidden_rows(at, t):
        cols_at, up_at = span(t, tile), pl.ds(pl.multiple_of(hid + t * tile, tile), tile)
        d_hidden = dot(routed[at, :], dw[cols_at, :], NT)
        gate, up = pre[at, cols_at], pre[at, up_at]
        sig = jax.nn.sigmoid(gate)
        act = gate * sig
        hidden[at, cols_at] = (act * up).astype(BF)
        dall[at, cols_at] = (d_hidden * up * sig * (1.0 + gate * (1.0 - sig))).astype(BF)
        dall[at, up_at] = (d_hidden * act).astype(BF)

    def hidden_group(at):
        pl.loop(0, hid // tile)(lambda t: hidden_rows(at, t))

    near = span(lax.div(me, half), half * cap)
    fars = [span(flip(lax.div(me, quarter), 2 + i, 4), quarter * cap) for i in range(2)]
    group = [*fars, near]
    hidden_group(near)

    @pl.loop(0, width // tile)
    def _(t):
        at = span(t, tile)
        xt[at, :] = x[:, at].T

    @pl.loop(half, half + quarter)
    def _(m):
        spread(m + 2)
        hand(m)

    z_copy(half, half).start()

    def back_part(at, block, out):
        @pl.loop(0, chan // tile)
        def _(t):
            cols_at = span(t, tile)
            value = dot(dall[at, :], w[span(block * (chan // tile) + t, tile), :], NT)
            parts[out, at, cols_at] = value.astype(BF)

    def sib_copy(g, i):
        return remote(
            parts.at[2 * i, group[g], :], from_sib.at[i, group[g], :],
            sib_sems.at[0, 2 * g + i], sib_sems.at[1, 2 * g + i], {"tp": sib},
        )

    def far_copy(m):
        at = row_at(flip(me, m, n_sp))
        return remote(far_out.at[at, :], far_in.at[at, :], far_sems.at[0, m], far_sems.at[1, m], {"tp": far})

    def ret_copy(m):
        to = flip(me, m, n_sp)
        return remote(
            final.at[row_at(to), :], back.at[row_at(me), :], ret_sems.at[0, m], ret_sems.at[1, m], {"sp": to}
        )

    def far_half(g, masks, between):
        at = group[g]
        back_part(at, far_sib, 0)
        sib_copy(g, 0).start()
        back_part(at, far, 1)
        between()
        sib_copy(g, 0).wait_recv()

        @pl.loop(*masks)
        def _(m):
            m = lax.rem(m, n_sp)
            r = row_at(flip(me, m, n_sp))
            far_out[r, :] = (parts[1, r, :].astype(F32) + from_sib[0, r, :].astype(F32)).astype(BF)
            far_copy(m).start()

    def near_half(g):
        at = group[g]
        back_part(at, sib, 2)
        sib_copy(g, 1).start()
        back_part(at, tp, 3)

    def finish_half(g):
        at = group[g]
        sib_copy(g, 1).wait_recv()
        total[at, :] = parts[3, at, :].astype(F32) + from_sib[1, at, :].astype(F32)

    def give(m):
        r = row_at(flip(me, m, n_sp))
        far_copy(m).wait_recv()
        final[r, :] = (total[r, :] + far_in[r, :].astype(F32)).astype(BF)
        ret_copy(m).start()

    def arrived(lo, hi):
        @pl.loop(lo, hi)
        def _(m):
            sib_share(m).wait_recv()
            hand_share(m).wait_recv()

    last = half + quarter
    arrived(half, last)
    hidden_group(fars[0])

    def hand_early():
        @pl.loop(last, n_sp)
        def _(m):
            if last + 2 < n_sp:
                pl.when(m + 2 < n_sp)(lambda: spread(m + 2))
            hand(m)

    far_half(0, (half, last), lambda: None)
    hand_early()
    near_half(0)
    arrived(last, n_sp)
    hidden_group(fars[1])
    far_half(1, (last, n_sp), lambda: None)
    for m in range(1, half):
        z_forward(m)
    finish_half(0)
    far_half(2, (1, half + 1) if half == n_sp else (1, half), lambda: None)
    r0 = row_at(me)
    far_out[r0, :] = (parts[1, r0, :].astype(F32) + from_sib[0, r0, :].astype(F32)).astype(BF)
    far_copy(0).start()
    pl.loop(half, last)(give)
    near_half(1)
    finish_half(1)
    pl.loop(last, n_sp)(give)
    near_half(2)
    finish_half(2)
    for m in range(half, n_sp):
        z_forward(m) if m == half else None

    chunks = width // tile
    each = -(-chunks // half)

    def in_chunk(i):
        at = span(i, tile)
        left = xt[at, :]
        ggrad[0, at, :] = (dot(left, dall[:, :hid], NN) * slot_scale).astype(BF)
        ugrad[0, at, :] = (dot(left, dall[:, hid:], NN) * slot_scale).astype(BF)

    def fill(i):
        for j in range(each):
            c = i * each + j
            if each * half > chunks:
                pl.when(c < chunks)(functools.partial(in_chunk, c))
            else:
                in_chunk(c)

    @pl.loop(1, half)
    def _(m):
        fill(m - 1)
        give(m)

    fill(half - 1)
    for m in range(half + 1, n_sp):
        z_forward(m)
    far_copy(0).wait_recv()
    back[r0, :] = (total[r0, :] + far_in[r0, :].astype(F32)).astype(BF)

    @pl.loop(0, hid // tile)
    def _(t):
        at = span(t, tile)
        dgrad[0, at, :] = (dot(hidden[:, at].T, routed[...], NN) * slot_scale).astype(BF)

    for load in loads[9:]:
        load.wait()

    @pl.loop(1, n_sp)
    def _(m):
        ret_copy(m).wait_recv()

    value = (grad[...].astype(F32) + dot(disp[...], back[...], NN)).astype(BF)
    resid[...] = value
    rfull[tp] = value
    close = remote(rfull.at[tp], rfull.at[tp], gat_sems.at[0], gat_sems.at[1], {"tp": sib})
    away = remote(rfull.at[tp], rfull.at[tp], gat_sems.at[2], gat_sems.at[3], {"tp": far})
    away.start()
    close.start()

    def e_copy(k, m):
        return remote(
            pieces.at[k, core], columns.at[me, core], e_sems.at[0, m], e_sems.at[1, m], {"sp": k}
        )

    def send_pieces(block):
        for j in range(per_block):
            k = block * per_block + j
            at = pl.ds(j * piece, piece)
            for c in range(2):
                pieces[k, c] = rfull[block, pl.ds(c * share, share), at]

            @pl.when(k != me)
            def _():
                e_copy(k, flip(me, k, n_sp)).start()

            @pl.when(k == me)
            def _():
                for c in range(2):
                    columns[me, c] = rfull[block, pl.ds(c * share, share), at]

    def mix_part(block):
        return dot(rfull[block], pw[span(block, chan), :], NN)

    send_pieces(tp)
    mix = mix_part(tp)
    close.wait_recv()
    send_pieces(sib)
    mix = mix + mix_part(sib)
    away.wait_recv()
    passed = remote(rfull.at[far], rfull.at[far], gat_sems.at[4], gat_sems.at[5], {"tp": sib})
    passed.start()
    send_pieces(far)
    mix = mix + mix_part(far)
    passed.wait_recv()
    send_pieces(far_sib)
    mix = mix + mix_part(far_sib)

    conv_grad = (mix * og[...].astype(F32)).astype(BF).astype(F32)
    edge_out[0] = jnp.broadcast_to(conv_grad[tokens - 1:tokens, :], edge_out.shape[1:])
    edge_out[1] = jnp.broadcast_to(conv_grad[0:1, :], edge_out.shape[1:])
    sides = [lax.rem(me + 1, n_sp), lax.rem(me + n_sp - 1, n_sp)]
    halos = [
        remote(edge_out.at[i], edge_in.at[i], halo_sems.at[0, i], halo_sems.at[1, i], {"sp": sides[i]})
        for i in range(2)
    ]
    for halo in halos:
        halo.start()
    og_out[...] = (mix * conv[...].astype(F32)).astype(BF)

    def e_share(m):
        at = columns.at[flip(me, m, n_sp), core]
        return remote(at, at, e_sems.at[2, m], e_sems.at[3, m], {"tp": sib})

    @pl.loop(1, n_sp)
    def _(m):
        e_copy(flip(me, m, n_sp), m).wait_recv()
        e_share(m).start()

    for halo in halos:
        halo.wait()
    before = jnp.where(me == 0, 0.0, edge_in[0, 0:1, :])
    after = jnp.where(me == n_sp - 1, 0.0, edge_in[1, 0:1, :])
    row = lax.broadcasted_iota(jnp.int32, (tokens, chan), 0)
    prev = jnp.where(row == 0, before, pltpu.roll(conv_grad, 1, 0))
    following = jnp.where(row == tokens - 1, after, pltpu.roll(conv_grad, tokens - 1, 0))
    tap = taps[...].astype(F32)
    value_grad = following * tap[0:1, :] + conv_grad * tap[1:2, :] + prev * tap[2:3, :]
    ig_out[...] = (value_grad * val[...].astype(F32)).astype(BF)
    val_out[...] = (value_grad * ig[...].astype(F32)).astype(BF)

    @pl.loop(0, n_sp)
    def _(m):
        far_share(m).wait_send()
        sib_share(m).wait_send()
        hand_share(m).wait_send()
        far_copy(m).wait_send()

    @pl.loop(1, n_sp)
    def _(m):
        sp_copy(m).wait_send()
        ret_copy(m).wait_send()
        e_copy(flip(me, m, n_sp), m).wait_send()
        e_share(m).wait_send()
        e_share(m).wait_recv()

    for g in range(3):
        for i in range(2):
            sib_copy(g, i).wait_send()
    for m in range(1, n_sp):
        z_copy(m, low(m)).wait_send()
        if low(m) == 1:
            z_copy(m, 1).wait_recv()
    for copy in (close, away, passed):
        copy.wait_send()


def finish_kernel(scale, columns, zall, *refs):
    grads, outs, proj, stage, sems = refs[:7], refs[7:14], refs[14], refs[15], refs[16]
    copies = [pltpu.make_async_copy(a, b, sems.at[i]) for i, (a, b) in enumerate(zip(grads, outs))]
    for copy in copies:
        copy.start()
    n_sp, parts, share, piece = columns.shape
    tokens = n_sp * parts * share
    left = columns[...].reshape(tokens, piece).T
    stage[...] = dot(left, zall[...].reshape(tokens, zall.shape[2]), NN) * scale
    last = pltpu.make_async_copy(stage, proj, sems.at[7])
    last.start()
    for copy in copies:
        copy.wait()
    last.wait()


def per_device(
    out_grad, route_ids, route_weight, expert_inputs, gate_weight, up_weight, down_weight,
    out_gate, in_gate, values, conv_out, conv_taps, proj_weight,
):
    n_sp, n_tp = lax.axis_size("sp"), lax.axis_size("tp")
    tokens, chan = out_grad.shape
    local, slots, width = expert_inputs.shape
    hid = gate_weight.shape[2]
    assert local == 1 and n_tp == 4 and n_sp & (n_sp - 1) == 0
    piece = width // n_sp
    dma = pltpu.SemaphoreType.DMA
    rows = jax.ShapeDtypeStruct((tokens, chan), BF)
    wide = jax.ShapeDtypeStruct((1, width, hid), BF)
    tall = jax.ShapeDtypeStruct((1, hid, width), BF)
    small = pltpu.VMEM((tokens, chan), BF)
    slab = pltpu.VMEM((slots, chan), BF)

    resid, og_out, ig_out, val_out, columns, zall, ggrad, ugrad, dgrad = pl.pallas_call(
        functools.partial(layer_kernel, n_sp, n_tp, n_sp * local, 1.0 / math.sqrt(slots)),
        out_shape=[
            rows, rows, rows, rows,
            jax.ShapeDtypeStruct((n_sp, 2, tokens // 2, piece), BF),
            jax.ShapeDtypeStruct((n_sp, tokens, chan), BF),
            wide, wide, tall,
        ],
        in_specs=[HBM] * 13,
        out_specs=[VMEM] * 9,
        scratch_shapes=[
            small,
            pltpu.VMEM((2, tokens), jnp.int32),
            pltpu.VMEM((2, tokens), F32),
            pltpu.VMEM((slots, width), BF),
            pltpu.VMEM((width, 2 * hid), BF),
            pltpu.VMEM((hid, width), BF),
            small, small, small, small,
            pltpu.VMEM(conv_taps.shape, BF),
            pltpu.VMEM(proj_weight.shape, BF),
            pltpu.VMEM((width, slots), BF),
            pltpu.VMEM((slots, 2 * hid), F32),
            pltpu.VMEM((slots, width), BF),
            pltpu.VMEM((slots, hid), BF),
            pltpu.VMEM((slots, 2 * hid), BF),
            slab,
            pltpu.VMEM((4, slots, chan), BF),
            pltpu.VMEM((2, slots, chan), BF),
            slab, slab,
            pltpu.VMEM((slots, chan), F32),
            slab, slab,
            pltpu.VMEM((tokens, slots), BF),
            pltpu.VMEM((n_tp, tokens, chan), BF),
            pltpu.VMEM((n_sp, 2, tokens // 2, piece), BF),
            pltpu.VMEM((2, 8, chan), F32),
            pltpu.VMEM((2, 8, chan), F32),
            dma((13,)), dma((8, n_sp)), dma((2, 6)), dma((2, n_sp)), dma((2, n_sp)), dma((6,)),
            dma((2, n_sp)), dma((4, n_sp)), dma((2, 2)),
        ],
        compiler_params=pltpu.CompilerParams(
            collective_id=0, has_side_effects=True, vmem_limit_bytes=44 * 2**20
        ),
        name="layer",
    )(*(
        pltpu.with_memory_space_constraint(a, pltpu.HBM) for a in (
            out_grad, route_ids.T, route_weight.T, expert_inputs, gate_weight, up_weight, down_weight,
            out_gate, in_gate, values, conv_out, conv_taps, proj_weight,
        )
    ))
    resid, og_out, ig_out, val_out, ggrad, ugrad, dgrad, proj_grad = pl.pallas_call(
        functools.partial(finish_kernel, 1.0 / math.sqrt(tokens * n_sp)),
        out_shape=[rows, rows, rows, rows, wide, wide, tall, jax.ShapeDtypeStruct((piece, chan), F32)],
        in_specs=[VMEM] * 9,
        out_specs=[HBM] * 8,
        scratch_shapes=[pltpu.VMEM((piece, chan), F32), dma((8,))],
        compiler_params=pltpu.CompilerParams(vmem_limit_bytes=6 * 2**20),
        name="finish",
    )(columns, zall, resid, og_out, ig_out, val_out, ggrad, ugrad, dgrad)
    return resid, og_out, ig_out, val_out, proj_grad, ggrad, ugrad, dgrad


def solution(mesh):
    rows = P("sp", "tp")
    in_specs = (
        rows, P("sp", None), P("sp", None), P("sp", None, None), P("sp", None, "tp"),
        P("sp", None, "tp"), P("sp", "tp", None), rows, rows, rows, rows, P(None, "tp"), P(None, "tp"),
    )
    out_specs = (
        rows, rows, rows, rows, rows, P("sp", None, "tp"), P("sp", None, "tp"), P("sp", "tp", None),
    )
    return jax.shard_map(
        per_device, mesh=mesh, in_specs=in_specs, out_specs=out_specs, check_vma=False
    )
```

time: 110 us -> 69.1 us (0.63); the launches traced: 108 us -> 69 us
  Pallas kernels: 83.5 us -> 66.4 us
  between operations: 14.1 us -> 0.65 us
  local copies, waits for them, and re-layouts: 6.45 us -> 1.88 us
  matrix products: 2.47 us -> 0 us
  other arithmetic: 1.66 us -> 0 us
    pallas_call x4 -> x2, Pallas kernels: 83.5 us -> 66.4 us  [the longest x1 62.4 us: per_device(): pl.pallas_call(functools.partial(layer_kernel, n_sp, n_tp, n_sp * local,...]
    unnamed x26 -> x2, local copies, waits for them, and re-layouts: 6.45 us -> 1.88 us
    dot_general x1 -> x0, matrix products: 2.47 us -> none  [per_device(): lax.dot_general(columns.reshape(n_sp * tokens, piece), mixed_all, (((0,),...]
    convert_element_type x1 -> x0, other arithmetic: 1.66 us -> none  [per_device(): mixed_in = (out_gate.astype(F32) * conv_out.astype(F32)).astype(BF)]
  transfers between devices with their start and end apart: 1 -> 0, of which waited for: 0 -> 0; matrix products, arithmetic and copies ran while one was open for 1% -> 0% of each run, Pallas kernels for 77% -> 0%
where the time goes in v1:
time: 69.1 us; the launch traced here: 69 us
  Pallas kernels  66.4 us (96%)
  local copies, waits for them, and re-layouts  1.88 us (3%)
    pallas_call x1, Pallas kernels, per_device(): pl.pallas_call(functools.partial(layer_kernel, n_sp, n_tp, n_sp * local,...  62.4 us
    pallas_call x1, Pallas kernels, per_device(): pl.pallas_call(functools.partial(finish_kernel, 1.0 / math.sqrt(tokens *...  4.07 us
    unnamed x2, local copies, waits for them, and re-layouts  1.88 us

profile of v1, /device:TPU:7, one launch (start us, length us, event | category | flops | bytes accessed | tf_op | source)
XLA Modules:
  0.0 69.0 jit_solution(4058428503542676374)
XLA Ops:
  0.6 62.4 %layer.1 = (bf16[128,512]{1,0:T(8,128)(2,1)S(1)}, bf16[128,512]{1,0:T(8,128)(2,1)S(1)}, bf16[128,512]{1,0:T(8,128)(2,1)S(1)}, bf16[128,512]{1,0:T(8,128)(2,1)S(1...) custom-call(bf16[128,512]{1,0:T(8,128)(2,1)} %grad_hbm.1, ...), custom_call_target="tpu_custom_call" | custom-call | tf_op jit(solution)/shard_map/layer/pallas_call | solution.py:511
  63.0 0.0 copy-start
  63.0 1.9 %copy-done = bf16[1,768,2048]{2,1,0:T(8,128)(2,1)S(1)} copy-done((bf16[1,768,2048]{2,1,0:T(8,128)(2,1)S(1)}, bf16[1,768,2048]{2,1,0:T(8,128)(2,1)}, u32[]{:S(2)}) %copy-start) | copy-done | bytes 3145752
  64.9 4.1 %finish.1 = (bf16[128,512]{1,0:T(8,128)(2,1)}, bf16[128,512]{1,0:T(8,128)(2,1)}, bf16[128,512]{1,0:T(8,128)(2,1)}, bf16[128,512]{1,0:T(8,128)(2,1)}, bf16[1,2048...) custom-call(bf16[8,2,64,256]{3,2,1,0:T(8,128)(2,1)S(1)} %get-tuple-eleme, ...), custom_call_target="tpu_custom_call" | custom-call | tf_op jit(solution)/shard_map/finish/pallas_call | solution.py:560
Async XLA Ops:
  63.0 1.9 %copy-start = (bf16[1,768,2048]{2,1,0:T(8,128)(2,1)S(1)}, bf16[1,768,2048]{2,1,0:T(8,128)(2,1)}, u32[]{:S(2)}) copy-start(bf16[1,768,2048]{2,1,0:T(8,128)(2,1)} %get-tuple-element.33.refs_6_) | copy-start | bytes 9437188

commit v2 on v1

v2 whole, which is shorter than its diff:
```python
import functools
import math

import jax
import jax.numpy as jnp
from jax import lax
from jax.experimental import pallas as pl
from jax.experimental.pallas import tpu as pltpu
from jax.sharding import PartitionSpec as P

BF = jnp.bfloat16
F32 = jnp.float32
MESH = pl.DeviceIdType.MESH
VMEM = pl.BlockSpec(memory_space=pltpu.VMEM)
HBM = pl.BlockSpec(memory_space=pltpu.HBM)
NN = ((1,), (0,))


def dot(left, right, dims):
    return lax.dot_general(left, right, (dims, ((), ())), preferred_element_type=F32)


def remote(src, dst, send, recv, device):
    return pltpu.make_async_remote_copy(
        src_ref=src, dst_ref=dst, send_sem=send, recv_sem=recv, device_id=device, device_id_type=MESH
    )


def span(index, size):
    return pl.ds(pl.multiple_of(index * size, size), size)


def flip(s, m, n):
    out, bit = 0, 1
    while bit < n:
        out = out + bit * lax.rem(lax.div(s, bit) + (m // bit if isinstance(m, int) else lax.div(m, bit)), 2)
        bit *= 2
    return out


def low(m):
    return m & -m


def layer_kernel(
    n_sp, n_tp, experts, slot_scale,
    grad_hbm, ids_hbm, rw_hbm, x_hbm, gw_hbm, uw_hbm, dw_hbm,
    og_hbm, ig_hbm, val_hbm, conv_hbm, taps_hbm, pw_hbm,
    resid, og_out, ig_out, val_out, columns, zall, ggrad, ugrad, dgrad,
    grad, ids, rw, x, og, ig, val, conv, taps, pw,
    wt, dt, pre, routed, hidden, dall, outgoing, parts, from_sib, far_out, far_in, total, final, back, disp,
    rfull, pieces, edge_out, edge_in,
    load_sems, send_sems, ex_recv, q_recv, sib_recv, far_recv, misc_recv, gat_sems, z_recv, e_recv,
    halo_sems,
):
    me, tp = lax.axis_index("sp"), lax.axis_index("tp")
    core = lax.rem(tp, 2)
    sib = tp + 1 - 2 * core
    far = lax.rem(tp + n_tp // 2, n_tp)
    far_sib = lax.rem(sib + n_tp // 2, n_tp)
    tokens, chan = grad.shape
    slots, width = x.shape
    hid = dgrad.shape[1]
    cap = slots // n_sp
    half, quarter = n_sp // 2, n_sp // 4
    piece = width // n_sp
    per_block = chan // piece
    share = tokens // 2
    tile = 256

    pairs = [
        (grad_hbm, grad), (ids_hbm, ids), (rw_hbm, rw), (og_hbm, og), (conv_hbm, conv),
        (x_hbm.at[0], x), (gw_hbm, ggrad), (uw_hbm, ugrad), (dw_hbm, dgrad), (ig_hbm, ig), (val_hbm, val), (taps_hbm, taps), (pw_hbm, pw),
    ]
    loads = [pltpu.make_async_copy(a, b, load_sems.at[i]) for i, (a, b) in enumerate(pairs)]
    for load in loads[:3]:
        load.start()
    barrier = pltpu.get_barrier_semaphore()
    for m in range(1, n_sp):
        pl.semaphore_signal(barrier, inc=1, device_id={"sp": flip(me, m, n_sp)}, device_id_type=MESH)
    for other in (sib, far):
        pl.semaphore_signal(barrier, inc=1, device_id={"tp": other}, device_id_type=MESH)
    for load in loads[3:]:
        load.start()
    for load in loads[:3]:
        load.wait()

    id0, id1 = ids[0:1, :], ids[1:2, :]
    names = lax.broadcasted_iota(jnp.int32, (experts, tokens), 0)
    hit0 = jnp.where(id0 == names, 1.0, 0.0).astype(F32)
    hit1 = jnp.where(id1 == names, 1.0, 0.0).astype(F32)
    rows = lax.broadcasted_iota(jnp.int32, (tokens, tokens), 0)
    cols = lax.broadcasted_iota(jnp.int32, (tokens, tokens), 1)
    earlier = jnp.where(rows < cols, 1.0, 0.0).astype(BF)
    counts = dot((hit0 + hit1).astype(BF), earlier, NN)
    slot0 = id0.astype(F32) * float(cap) + jnp.sum(counts * hit0, axis=0, keepdims=True)
    slot1 = id1.astype(F32) * float(cap) + jnp.sum(counts * hit1, axis=0, keepdims=True)
    places = lax.broadcasted_iota(jnp.int32, (experts * cap, tokens), 0).astype(F32)
    at0, at1 = slot0 == places, slot1 == places
    weight = jnp.sum(
        jnp.where(at0, rw[0:1, :], 0.0) + jnp.where(at1, rw[1:2, :], 0.0), axis=1, keepdims=True
    )
    chosen = (jnp.where(at0, 1.0, 0.0) + jnp.where(at1, 1.0, 0.0)).astype(BF)
    outgoing[...] = (dot(chosen, grad[...], NN) * weight).astype(BF)

    pl.semaphore_wait(barrier, n_sp + 1)

    def row_at(s):
        return span(s, cap)

    def place(j, s):
        return routed.at[row_at(s), span(j, chan)]

    def sent(i, ref):
        return remote(ref, ref, send_sems.at[i], q_recv.at[0, 0], {"tp": sib})

    def taken(ref, sem):
        return remote(ref, ref, send_sems.at[0], sem, {"tp": sib})

    def sp_copy(m):
        to = flip(me, m, n_sp)
        return remote(
            outgoing.at[row_at(to), :], place(tp, me), send_sems.at[0], ex_recv.at[0, m], {"sp": to}
        )

    def far_share(m):
        at = place(tp, flip(me, m, n_sp))
        return remote(at, at, send_sems.at[1], ex_recv.at[1, m], {"tp": far})

    def sib_share(m):
        at = place(tp, flip(me, m, n_sp))
        return remote(at, at, send_sems.at[2], q_recv.at[0, lax.div(m, quarter)], {"tp": sib})

    def hand_share(m):
        at = place(far, flip(me, m, n_sp))
        return remote(at, at, send_sems.at[3], q_recv.at[1, lax.div(m, quarter)], {"tp": sib})

    def spread(m):
        sp_copy(m).wait_recv()
        far_share(m).start()
        sib_share(m).start()

    def hand(m):
        far_share(m).wait_recv()
        hand_share(m).start()

    @pl.loop(1, n_sp)
    def _(m):
        sp_copy(m).start()

    own = pltpu.make_async_copy(outgoing.at[row_at(me), :], place(tp, me), ex_recv.at[0, 0])
    own.start()
    own.wait()
    far_share(jnp.int32(0)).start()
    sib_share(jnp.int32(0)).start()

    loads[3].wait()
    loads[4].wait()
    zall[me] = (og[...].astype(F32) * conv[...].astype(F32)).astype(BF)
    disp[...] = chosen.T

    def z_copy(result, bit):
        block = flip(me, result - bit, n_sp)
        return remote(
            zall.at[block], zall.at[block], send_sems.at[7], z_recv.at[result],
            {"sp": flip(me, bit, n_sp)},
        )

    def z_send(m):
        bit = low(m) // 2 if m else half
        while bit:
            z_copy(m + bit, bit).start()
            bit //= 2

    def z_forward(m):
        if low(m) > 1:
            z_copy(m, low(m)).wait_recv()
            z_send(m)

    def pre_dot(t):
        at, up_at = span(t, tile), pl.ds(pl.multiple_of(hid + t * tile, tile), tile)
        pre[:, at] = dot(x[...], ggrad[0, :, at], NN)
        pre[:, up_at] = dot(x[...], ugrad[0, :, at], NN)

    for load in loads[6:8]:
        load.wait()
    def turn(i):
        at = span(i, tile)
        wt[:hid, at] = ggrad[0, at, :].T
        wt[hid:, at] = ugrad[0, at, :].T

    pre_tiles = hid // tile

    def prepare(t):
        pre_dot(t)
        dt[:, span(t, tile)] = dgrad[0, span(t, tile), :].T

    def each(lo, hi, step):
        if lo < hi:
            pl.loop(lo, hi)(step)

    bit, last = quarter // 2, half + quarter
    each(0, width // tile, turn)
    for load in (loads[5], loads[8]):
        load.wait()
    each(1, quarter, spread)
    each(0, min(1, pre_tiles), prepare)
    each(quarter, half, spread)
    each(0, bit, hand)
    each(1, min(2, pre_tiles), prepare)
    each(bit, quarter, hand)
    each(half, half + bit, spread)
    each(2, pre_tiles, prepare)
    each(quarter, quarter + bit, hand)
    each(half + bit, last, spread)
    each(quarter + bit, half, hand)

    def hidden_group(at):
        d_hidden = dot(routed[at, :], dt[...], NN)
        gate, up = pre[at, :hid], pre[at, hid:]
        sig = jax.nn.sigmoid(gate)
        act = gate * sig
        hidden[at, :] = (act * up).astype(BF)
        dall[at, :hid] = (d_hidden * up * sig * (1.0 + gate * (1.0 - sig))).astype(BF)
        dall[at, hid:] = (d_hidden * act).astype(BF)

    def arrived(q):
        for i in range(2):
            taken(outgoing.at[pl.ds(0, quarter * cap), :], q_recv.at[i, q]).wait_recv()

    near = span(lax.div(me, half), half * cap)
    fars = [span(flip(lax.div(me, quarter), 2 + i, 4), quarter * cap) for i in range(2)]
    group = [*fars, near]
    arrived(0)
    arrived(1)
    hidden_group(near)
    z_send(0)
    each(half, last, hand)
    each(last, last + bit, spread)

    def back_part(at, block, out):
        parts[out, at, :] = dot(dall[at, :], wt[:, span(block, chan)], NN).astype(BF)

    def sib_copy(g, i):
        return remote(
            parts.at[2 * i, group[g], :], from_sib.at[i, group[g], :],
            send_sems.at[4], sib_recv.at[2 * g + i], {"tp": sib},
        )

    side = chan // 2
    sides = [pl.ds(0, side), pl.ds(side, side)]

    def far_copy(m, h):
        at = row_at(flip(me, m, n_sp))
        return remote(
            far_out.at[at, sides[h]], far_in.at[at, sides[h]],
            send_sems.at[5], far_recv.at[h, m], {"tp": far},
        )

    def ret_copy(m, h):
        to = flip(me, m, n_sp)
        return remote(
            final.at[row_at(to), sides[h]], back.at[row_at(me), sides[h]],
            send_sems.at[6], misc_recv.at[h], {"sp": to},
        )

    def parts_of(g, i, others):
        for j in range(2):
            back_part(group[g], others[j], 2 * i + j)
            if j == 0:
                sib_copy(g, i).start()

    def push(m, h):
        r, c = row_at(flip(me, m, n_sp)), sides[h]
        far_out[r, c] = (parts[1, r, c].astype(F32) + from_sib[0, r, c].astype(F32)).astype(BF)
        far_copy(m, h).start()

    push0, push1 = (functools.partial(push, h=h) for h in range(2))

    def add_up(g):
        at = group[g]
        sib_copy(g, 1).wait_recv()
        total[at, :] = parts[3, at, :].astype(F32) + from_sib[1, at, :].astype(F32)

    def summed(r, h):
        return (total[r, sides[h]] + far_in[r, sides[h]].astype(F32)).astype(BF)

    def give(m, h):
        r = row_at(flip(me, m, n_sp))
        far_copy(m, h).wait_recv()
        final[r, sides[h]] = summed(r, h)
        ret_copy(m, h).start()

    give0, give1 = (functools.partial(give, h=h) for h in range(2))

    away_parts, home_parts = (far_sib, far), (sib, tp)
    arrived(2)
    hidden_group(fars[0])
    each(last + bit, n_sp, spread)
    parts_of(0, 0, away_parts)
    sib_copy(0, 0).wait_recv()
    each(half, last, push0)
    each(half, last, push1)
    parts_of(0, 1, home_parts)
    each(last, last + bit, hand)
    parts_of(2, 0, away_parts)
    each(last + bit, n_sp, hand)
    sib_copy(2, 0).wait_recv()
    each(1, half, push0)
    add_up(0)
    arrived(3)
    hidden_group(fars[1])
    each(half, last, give0)
    parts_of(1, 0, away_parts)
    each(half, last, give1)
    sib_copy(1, 0).wait_recv()
    each(last, n_sp, push0)
    push0(0)
    each(last, n_sp, push1)
    each(1, half, push1)
    push1(0)
    for m in range(1, half):
        z_forward(m)
    parts_of(1, 1, home_parts)
    parts_of(2, 1, home_parts)
    add_up(2)
    add_up(1)

    chunks = width // tile
    count = -(-chunks // half)

    def in_chunk(i):
        at = span(i, tile)
        left = x[:, at].T
        ggrad[0, at, :] = (dot(left, dall[:, :hid], NN) * slot_scale).astype(BF)
        ugrad[0, at, :] = (dot(left, dall[:, hid:], NN) * slot_scale).astype(BF)

    def fill(i):
        for j in range(count):
            c = i * count + j
            if count * half > chunks:
                pl.when(c < chunks)(functools.partial(in_chunk, c))
            else:
                in_chunk(c)

    def keep(h):
        r0 = row_at(me)
        far_copy(0, h).wait_recv()
        back[r0, sides[h]] = summed(r0, h)

    each(1, half, give0)
    fill(0)
    each(last, n_sp, give0)
    keep(0)
    fill(1)
    each(last, n_sp, give1)
    each(2, half - 1, fill)
    each(1, half, give1)
    keep(1)
    z_forward(half)
    fill(half - 1)

    for load in loads[9:]:
        load.wait()

    mine = span(core, share)

    def copy_block(block, h, i, other):
        ref = rfull.at[block, :, sides[h]]
        return remote(ref, ref, gat_sems.at[0, 3 * h + i], gat_sems.at[1, 3 * h + i], {"tp": other})

    away = [copy_block(tp, h, 0, far) for h in range(2)]
    close = [copy_block(tp, h, 1, sib) for h in range(2)]
    passed = [copy_block(far, h, 2, sib) for h in range(2)]

    def e_copy(k, m):
        return remote(pieces.at[k], columns.at[me, core], send_sems.at[8], e_recv.at[m], {"sp": k})

    def send_pieces(block, h):
        for j in range(h * per_block // 2, (h + 1) * per_block // 2):
            k = block * per_block + j
            pieces[k] = rfull[block, mine, pl.ds(j * piece, piece)]

            @pl.when(k != me)
            def _():
                e_copy(k, flip(me, k, n_sp)).start()

    def combine(h):
        c = sides[h]
        taken(outgoing.at[pl.ds(0, (n_sp - 1) * cap), c], misc_recv.at[h]).wait_recv()
        value = (grad[:, c].astype(F32) + dot(disp[...], back[:, c], NN)).astype(BF)
        resid[:, c] = value
        rfull[tp, :, c] = value
        away[h].start()
        close[h].start()
        send_pieces(tp, h)

    def mix_part(block):
        return dot(rfull[block], pw[span(block, chan), :], NN)

    def down_chunk(t):
        at = span(t, tile)
        dgrad[0, at, :] = (dot(hidden[:, at].T, routed[...], NN) * slot_scale).astype(BF)

    combine(0)
    pl.loop(0, hid // tile)(down_chunk)
    close[0].wait_recv()
    send_pieces(sib, 0)
    combine(1)
    mix = mix_part(tp)
    away[0].wait_recv()
    passed[0].start()
    send_pieces(far, 0)
    passed[0].wait_recv()
    send_pieces(far_sib, 0)
    for m in range(half + 1, n_sp):
        z_forward(m)
    close[1].wait_recv()
    send_pieces(sib, 1)
    mix = mix + mix_part(sib)
    away[1].wait_recv()
    passed[1].start()
    send_pieces(far, 1)
    mix = mix + mix_part(far)
    passed[1].wait_recv()
    send_pieces(far_sib, 1)
    mix = mix + mix_part(far_sib)
    for j in range(per_block):
        @pl.when(lax.rem(me, per_block) == j)
        def _():
            for c in range(2):
                columns[me, c] = rfull[
                    lax.div(me, per_block), pl.ds(c * share, share), pl.ds(j * piece, piece)
                ]

    conv_grad = (mix * og[...].astype(F32)).astype(BF).astype(F32)
    edge_out[0] = jnp.broadcast_to(conv_grad[tokens - 1:tokens, :], edge_out.shape[1:])
    edge_out[1] = jnp.broadcast_to(conv_grad[0:1, :], edge_out.shape[1:])
    ends = [lax.rem(me + 1, n_sp), lax.rem(me + n_sp - 1, n_sp)]
    halos = [
        remote(edge_out.at[i], edge_in.at[i], halo_sems.at[0, i], halo_sems.at[1, i], {"sp": ends[i]})
        for i in range(2)
    ]
    for halo in halos:
        halo.start()
    og_out[...] = (mix * conv[...].astype(F32)).astype(BF)

    def e_share(m):
        at = columns.at[flip(me, m, n_sp), core]
        return remote(at, at, send_sems.at[9], misc_recv.at[2], {"tp": sib})

    @pl.loop(1, n_sp)
    def _(m):
        e_copy(flip(me, m, n_sp), m).wait_recv()
        e_share(m).start()

    for halo in halos:
        halo.wait()
    before = jnp.where(me == 0, 0.0, edge_in[0, 0:1, :])
    after = jnp.where(me == n_sp - 1, 0.0, edge_in[1, 0:1, :])
    row = lax.broadcasted_iota(jnp.int32, (tokens, chan), 0)
    prev = jnp.where(row == 0, before, pltpu.roll(conv_grad, 1, 0))
    following = jnp.where(row == tokens - 1, after, pltpu.roll(conv_grad, tokens - 1, 0))
    tap = taps[...].astype(F32)
    value_grad = following * tap[0:1, :] + conv_grad * tap[1:2, :] + prev * tap[2:3, :]
    ig_out[...] = (value_grad * val[...].astype(F32)).astype(BF)
    val_out[...] = (value_grad * ig[...].astype(F32)).astype(BF)

    less = outgoing.at[pl.ds(0, (n_sp - 1) * cap), :]
    block = columns.at[pl.ds(0, n_sp - 1), 0]
    slices = [
        less, outgoing, outgoing, outgoing, from_sib, outgoing, less,
        zall.at[pl.ds(0, n_sp - 1)], pieces.at[pl.ds(0, n_sp - 1)], block,
    ]
    for i, ref in enumerate(slices):
        sent(i, ref).wait_send()
    taken(block, misc_recv.at[2]).wait_recv()
    for m in range(1, n_sp, 2):
        z_copy(m, 1).wait_recv()
    for copy in (*away, *close, *passed):
        copy.wait_send()


def finish_kernel(scale, columns, zall, *refs):
    grads, outs, proj, stage, sems = refs[:7], refs[7:14], refs[14], refs[15], refs[16]
    copies = [pltpu.make_async_copy(a, b, sems.at[i]) for i, (a, b) in enumerate(zip(grads, outs))]
    for copy in copies:
        copy.start()
    n_sp, parts, share, piece = columns.shape
    tokens = n_sp * parts * share
    left = columns[...].reshape(tokens, piece).T
    stage[...] = dot(left, zall[...].reshape(tokens, zall.shape[2]), NN) * scale
    last = pltpu.make_async_copy(stage, proj, sems.at[7])
    last.start()
    for copy in copies:
        copy.wait()
    last.wait()


def per_device(
    out_grad, route_ids, route_weight, expert_inputs, gate_weight, up_weight, down_weight,
    out_gate, in_gate, values, conv_out, conv_taps, proj_weight,
):
    n_sp, n_tp = lax.axis_size("sp"), lax.axis_size("tp")
    tokens, chan = out_grad.shape
    local, slots, width = expert_inputs.shape
    hid = gate_weight.shape[2]
    assert local == 1 and n_tp == 4 and n_sp & (n_sp - 1) == 0
    piece = width // n_sp
    dma = pltpu.SemaphoreType.DMA
    rows = jax.ShapeDtypeStruct((tokens, chan), BF)
    wide = jax.ShapeDtypeStruct((1, width, hid), BF)
    tall = jax.ShapeDtypeStruct((1, hid, width), BF)
    small = pltpu.VMEM((tokens, chan), BF)
    slab = pltpu.VMEM((slots, chan), BF)

    resid, og_out, ig_out, val_out, columns, zall, ggrad, ugrad, dgrad = pl.pallas_call(
        functools.partial(layer_kernel, n_sp, n_tp, n_sp * local, 1.0 / math.sqrt(slots)),
        out_shape=[
            rows, rows, rows, rows,
            jax.ShapeDtypeStruct((n_sp, 2, tokens // 2, piece), BF),
            jax.ShapeDtypeStruct((n_sp, tokens, chan), BF),
            wide, wide, tall,
        ],
        in_specs=[HBM] * 13,
        out_specs=[VMEM] * 9,
        scratch_shapes=[
            small,
            pltpu.VMEM((2, tokens), jnp.int32),
            pltpu.VMEM((2, tokens), F32),
            pltpu.VMEM((slots, width), BF),
            small, small, small, small,
            pltpu.VMEM(conv_taps.shape, BF),
            pltpu.VMEM(proj_weight.shape, BF),
            pltpu.VMEM((2 * hid, width), BF),
            pltpu.VMEM((width, hid), BF),
            pltpu.VMEM((slots, 2 * hid), F32),
            pltpu.VMEM((slots, width), BF),
            pltpu.VMEM((slots, hid), BF),
            pltpu.VMEM((slots, 2 * hid), BF),
            slab,
            pltpu.VMEM((4, slots, chan), BF),
            pltpu.VMEM((2, slots, chan), BF),
            slab, slab,
            pltpu.VMEM((slots, chan), F32),
            slab, slab,
            pltpu.VMEM((tokens, slots), BF),
            pltpu.VMEM((n_tp, tokens, chan), BF),
            pltpu.VMEM((n_sp, tokens // 2, piece), BF),
            pltpu.VMEM((2, 8, chan), F32),
            pltpu.VMEM((2, 8, chan), F32),
            dma((13,)), dma((10,)), dma((2, n_sp)), dma((2, 4)), dma((6,)), dma((2, n_sp)), dma((3,)),
            dma((2, 6)), dma((n_sp,)), dma((n_sp,)), dma((2, 2)),
        ],
        compiler_params=pltpu.CompilerParams(
            collective_id=0, has_side_effects=True, vmem_limit_bytes=38 * 2**20
        ),
        name="layer",
    )(*(
        pltpu.with_memory_space_constraint(a, pltpu.HBM) for a in (
            out_grad, route_ids.T, route_weight.T, expert_inputs, gate_weight, up_weight, down_weight,
            out_gate, in_gate, values, conv_out, conv_taps, proj_weight,
        )
    ))
    resid, og_out, ig_out, val_out, ggrad, ugrad, dgrad, proj_grad = pl.pallas_call(
        functools.partial(finish_kernel, 1.0 / math.sqrt(tokens * n_sp)),
        out_shape=[rows, rows, rows, rows, wide, wide, tall, jax.ShapeDtypeStruct((piece, chan), F32)],
        in_specs=[VMEM] * 9,
        out_specs=[HBM] * 8,
        scratch_shapes=[pltpu.VMEM((piece, chan), F32), dma((8,))],
        compiler_params=pltpu.CompilerParams(vmem_limit_bytes=6 * 2**20),
        name="finish",
    )(columns, zall, resid, og_out, ig_out, val_out, ggrad, ugrad, dgrad)
    return resid, og_out, ig_out, val_out, proj_grad, ggrad, ugrad, dgrad


def solution(mesh):
    rows = P("sp", "tp")
    in_specs = (
        rows, P("sp", None), P("sp", None), P("sp", None, None), P("sp", None, "tp"),
        P("sp", None, "tp"), P("sp", "tp", None), rows, rows, rows, rows, P(None, "tp"), P(None, "tp"),
    )
    out_specs = (
        rows, rows, rows, rows, rows, P("sp", None, "tp"), P("sp", None, "tp"), P("sp", "tp", None),
    )
    return jax.shard_map(
        per_device, mesh=mesh, in_specs=in_specs, out_specs=out_specs, check_vma=False
    )
```

time: 69.1 us -> 56.9 us (0.82)
  Pallas kernels: 66.4 us -> 56 us
  local copies, waits for them, and re-layouts: 1.88 us -> 0 us
    pallas_call x1, Pallas kernels: 62.4 us -> 51.9 us  [per_device(): pl.pallas_call(functools.partial(layer_kernel, n_sp, n_tp, n_sp * local,...]
    unnamed x2 -> x0, local copies, waits for them, and re-layouts: 1.88 us -> none
where the time goes in v2:
time: 56.9 us; the launch traced here: 56.8 us
  Pallas kernels  56 us (98%)
  between operations  0.81 us (1%)
    pallas_call x1, Pallas kernels, per_device(): pl.pallas_call(functools.partial(layer_kernel, n_sp, n_tp, n_sp * local,...  51.9 us
    pallas_call x1, Pallas kernels, per_device(): pl.pallas_call(functools.partial(finish_kernel, 1.0 / math.sqrt(tokens *...  4.07 us

profile of v2, /device:TPU:7, one launch (start us, length us, event | category | flops | bytes accessed | tf_op | source)
XLA Modules:
  0.0 56.8 jit_solution(3738013175089874013)
XLA Ops:
  0.6 51.9 %layer.1 = (bf16[128,512]{1,0:T(8,128)(2,1)S(1)}, bf16[128,512]{1,0:T(8,128)(2,1)S(1)}, bf16[128,512]{1,0:T(8,128)(2,1)S(1)}, bf16[128,512]{1,0:T(8,128)(2,1)S(1...) custom-call(bf16[128,512]{1,0:T(8,128)(2,1)} %grad_hbm.1, ...), custom_call_target="tpu_custom_call" | custom-call | tf_op jit(solution)/shard_map/layer/pallas_call | solution.py:517
  52.6 4.1 %finish.1 = (bf16[128,512]{1,0:T(8,128)(2,1)}, bf16[128,512]{1,0:T(8,128)(2,1)}, bf16[128,512]{1,0:T(8,128)(2,1)}, bf16[128,512]{1,0:T(8,128)(2,1)}, bf16[1,2048...) custom-call(bf16[8,2,64,256]{3,2,1,0:T(8,128)(2,1)S(1)} %get-tuple-eleme, ...), custom_call_target="tpu_custom_call" | custom-call | tf_op jit(solution)/shard_map/finish/pallas_call | solution.py:565

commit v3 on v2

--- a/solution.py
+++ b/solution.py
@@ -69,8 +69,9 @@
     tile = 256
 
     pairs = [
-        (grad_hbm, grad), (ids_hbm, ids), (rw_hbm, rw), (og_hbm, og), (conv_hbm, conv),
-        (x_hbm.at[0], x), (gw_hbm, ggrad), (uw_hbm, ugrad), (dw_hbm, dgrad), (ig_hbm, ig), (val_hbm, val), (taps_hbm, taps), (pw_hbm, pw),
+        (grad_hbm, grad), (ids_hbm, ids), (rw_hbm, rw), (gw_hbm, ggrad), (uw_hbm, ugrad),
+        (x_hbm.at[0], x), (dw_hbm, dgrad), (og_hbm, og), (conv_hbm, conv),
+        (ig_hbm, ig), (val_hbm, val), (taps_hbm, taps), (pw_hbm, pw),
     ]
     loads = [pltpu.make_async_copy(a, b, load_sems.at[i]) for i, (a, b) in enumerate(pairs)]
     for load in loads[:3]:
@@ -144,19 +145,17 @@
         far_share(m).wait_recv()
         hand_share(m).start()
 
-    @pl.loop(1, n_sp)
-    def _(m):
+    def dispatch(m):
         sp_copy(m).start()
 
+    last = half + quarter
+    pl.loop(1, last)(dispatch)
     own = pltpu.make_async_copy(outgoing.at[row_at(me), :], place(tp, me), ex_recv.at[0, 0])
     own.start()
     own.wait()
     far_share(jnp.int32(0)).start()
     sib_share(jnp.int32(0)).start()
 
-    loads[3].wait()
-    loads[4].wait()
-    zall[me] = (og[...].astype(F32) * conv[...].astype(F32)).astype(BF)
     disp[...] = chosen.T
 
     def z_copy(result, bit):
@@ -182,7 +181,7 @@
         pre[:, at] = dot(x[...], ggrad[0, :, at], NN)
         pre[:, up_at] = dot(x[...], ugrad[0, :, at], NN)
 
-    for load in loads[6:8]:
+    for load in loads[3:5]:
         load.wait()
     def turn(i):
         at = span(i, tile)
@@ -199,20 +198,21 @@
         if lo < hi:
             pl.loop(lo, hi)(step)
 
-    bit, last = quarter // 2, half + quarter
+    bit = quarter // 2
     each(0, width // tile, turn)
-    for load in (loads[5], loads[8]):
+    for load in loads[5:7]:
         load.wait()
     each(1, quarter, spread)
     each(0, min(1, pre_tiles), prepare)
+    pl.loop(last, n_sp)(dispatch)
     each(quarter, half, spread)
     each(0, bit, hand)
+    each(half, half + bit, spread)
     each(1, min(2, pre_tiles), prepare)
     each(bit, quarter, hand)
-    each(half, half + bit, spread)
+    each(half + bit, last, spread)
+    each(quarter, quarter + bit, hand)
     each(2, pre_tiles, prepare)
-    each(quarter, quarter + bit, hand)
-    each(half + bit, last, spread)
     each(quarter + bit, half, hand)
 
     def hidden_group(at):
@@ -234,6 +234,9 @@
     arrived(0)
     arrived(1)
     hidden_group(near)
+    for load in loads[7:9]:
+        load.wait()
+    zall[me] = (og[...].astype(F32) * conv[...].astype(F32)).astype(BF)
     z_send(0)
     each(half, last, hand)
     each(last, last + bit, spread)
@@ -411,10 +414,10 @@
     away[0].wait_recv()
     passed[0].start()
     send_pieces(far, 0)
+    for m in range(half + 1, n_sp):
+        z_forward(m)
     passed[0].wait_recv()
     send_pieces(far_sib, 0)
-    for m in range(half + 1, n_sp):
-        z_forward(m)
     close[1].wait_recv()
     send_pieces(sib, 1)
     mix = mix + mix_part(sib)
@@ -484,7 +487,13 @@
 def finish_kernel(scale, columns, zall, *refs):
     grads, outs, proj, stage, sems = refs[:7], refs[7:14], refs[14], refs[15], refs[16]
     copies = [pltpu.make_async_copy(a, b, sems.at[i]) for i, (a, b) in enumerate(zip(grads, outs))]
-    for copy in copies:
+    cuts = 8
+    for i in range(4, 7):
+        rows = grads[i].shape[1] // cuts
+        for c in range(cuts):
+            at = pl.ds(c * rows, rows)
+            pltpu.make_async_copy(grads[i].at[:, at], outs[i].at[:, at], sems.at[i]).start()
+    for copy in copies[:4]:
         copy.start()
     n_sp, parts, share, piece = columns.shape
     tokens = n_sp * parts * share

time: 56.9 us -> 56.2 us (0.988); the launches traced: 56.8 us -> 55.3 us
  Pallas kernels: 56 us -> 54.5 us
    pallas_call x1, Pallas kernels: 51.9 us -> 50.5 us  [per_device(): pl.pallas_call(functools.partial(layer_kernel, n_sp, n_tp, n_sp * local,...]
where the time goes in v3:
time: 56.2 us; the launch traced here: 55.3 us
  Pallas kernels  54.5 us (97%)
  between operations  0.81 us (1%)
    pallas_call x1, Pallas kernels, per_device(): pl.pallas_call(functools.partial(layer_kernel, n_sp, n_tp, n_sp * local,...  50.5 us
    pallas_call x1, Pallas kernels, per_device(): pl.pallas_call(functools.partial(finish_kernel, 1.0 / math.sqrt(tokens *...  4 us

profile of v3, /device:TPU:7, one launch (start us, length us, event | category | flops | bytes accessed | tf_op | source)
XLA Modules:
  0.0 55.3 jit_solution(17096823070093549242)
XLA Ops:
  0.6 50.5 %layer.1 = (bf16[128,512]{1,0:T(8,128)(2,1)S(1)}, bf16[128,512]{1,0:T(8,128)(2,1)S(1)}, bf16[128,512]{1,0:T(8,128)(2,1)S(1)}, bf16[128,512]{1,0:T(8,128)(2,1)S(1...) custom-call(bf16[128,512]{1,0:T(8,128)(2,1)} %grad_hbm.1, ...), custom_call_target="tpu_custom_call" | custom-call | tf_op jit(solution)/shard_map/layer/pallas_call | solution.py:526
  51.1 4.0 %finish.1 = (bf16[128,512]{1,0:T(8,128)(2,1)}, bf16[128,512]{1,0:T(8,128)(2,1)}, bf16[128,512]{1,0:T(8,128)(2,1)}, bf16[128,512]{1,0:T(8,128)(2,1)}, bf16[1,2048...) custom-call(bf16[8,2,64,256]{3,2,1,0:T(8,128)(2,1)S(1)} %get-tuple-eleme, ...), custom_call_target="tpu_custom_call" | custom-call | tf_op jit(solution)/shard_map/finish/pallas_call | solution.py:574

commit v4 on v3

--- a/solution.py
+++ b/solution.py
@@ -204,8 +204,8 @@
         load.wait()
     each(1, quarter, spread)
     each(0, min(1, pre_tiles), prepare)
+    each(quarter, half, spread)
     pl.loop(last, n_sp)(dispatch)
-    each(quarter, half, spread)
     each(0, bit, hand)
     each(half, half + bit, spread)
     each(1, min(2, pre_tiles), prepare)

time: 56.2 us -> 55.6 us (0.989); the launches traced: 55.3 us -> 55.5 us
  no operation moved by 1% of the time
where the time goes in v4:
time: 55.6 us; the launch traced here: 55.5 us
  Pallas kernels  54.6 us (98%)
  between operations  0.81 us (1%)
    pallas_call x1, Pallas kernels, per_device(): pl.pallas_call(functools.partial(layer_kernel, n_sp, n_tp, n_sp * local,...  50.7 us
    pallas_call x1, Pallas kernels, per_device(): pl.pallas_call(functools.partial(finish_kernel, 1.0 / math.sqrt(tokens *...  4 us

profile of v4, /device:TPU:7, one launch (start us, length us, event | category | flops | bytes accessed | tf_op | source)
XLA Modules:
  0.0 55.5 jit_solution(8648103618730291012)
XLA Ops:
  0.6 50.7 %layer.1 = (bf16[128,512]{1,0:T(8,128)(2,1)S(1)}, bf16[128,512]{1,0:T(8,128)(2,1)S(1)}, bf16[128,512]{1,0:T(8,128)(2,1)S(1)}, bf16[128,512]{1,0:T(8,128)(2,1)S(1...) custom-call(bf16[128,512]{1,0:T(8,128)(2,1)} %grad_hbm.1, ...), custom_call_target="tpu_custom_call" | custom-call | tf_op jit(solution)/shard_map/layer/pallas_call | solution.py:526
  51.3 4.0 %finish.1 = (bf16[128,512]{1,0:T(8,128)(2,1)}, bf16[128,512]{1,0:T(8,128)(2,1)}, bf16[128,512]{1,0:T(8,128)(2,1)}, bf16[128,512]{1,0:T(8,128)(2,1)}, bf16[1,2048...) custom-call(bf16[8,2,64,256]{3,2,1,0:T(8,128)(2,1)S(1)} %get-tuple-eleme, ...), custom_call_target="tpu_custom_call" | custom-call | tf_op jit(solution)/shard_map/finish/pallas_call | solution.py:574
